TPU v7x, 32 devices: a whole 2x2x4 slice. The times are simulated.
32 devices in a mesh: sp: 16 (over z, y, x), dp: 2 (over core).
Axes of the slice: x: 2, y: 2, z: 4, core: 2. Of those that a mesh axis runs over, the one named last changes fastest.
Arguments:
- glu_value: bfloat16 [2, 8192, 512], P('dp', 'sp'), may hold values from -6 to 6
- glu_gate: bfloat16 [2, 8192, 512], P('dp', 'sp'), may hold values from -8 to 8
- cotangent: bfloat16 [2, 8192, 2048], P('dp', 'sp'), may hold values from -8 to 8
- conv_weight: float32 [31, 512], replicated, may hold values from -1 to 1
- norm_gain: float32 [512], replicated, may hold values from 0.1 to 1.9
- norm_shift: float32 [512], replicated, may hold values from -3 to 3
- out_weight: bfloat16 [2048, 512], P('dp'), may hold values from -0.25 to 0.25
Outputs:
- grad_value: bfloat16 [2, 8192, 512], P('dp', 'sp')
- grad_gate: bfloat16 [2, 8192, 512], P('dp', 'sp')
- grad_out_weight: float32 [2048, 512], P('dp')
- grad_conv: float32 [31, 512], replicated
- grad_gain: float32 [512], replicated
- grad_shift: float32 [512], replicated
All inputs are finite; a program needn't handle non-finite values.
Results may differ from a plain program's by a relative error of at most 0.003.
Values may be sent and summed in bfloat16 or wider, within the bound.
A program may use at most 64 MiB of HBM per device.

v0:
```python
import math

import jax
import jax.numpy as jnp
from jax import lax
from jax.sharding import PartitionSpec as P

epsilon = 1e-06


def from_behind(value, axis, by):
    count = lax.axis_size(axis)
    pairs = [(i, i + by) for i in range(count) if 0 <= i + by < count]
    return lax.ppermute(value, axis, pairs)


def per_device(glu_value, glu_gate, cotangent, conv_weight, norm_gain, norm_shift, out_weight):
    value_rows = glu_value[0]
    gate_rows = glu_gate[0]
    cotan_rows = cotangent[0]
    length = value_rows.shape[0]
    channels = value_rows.shape[1]
    tap_count = conv_weight.shape[0]
    halo_rows = tap_count - 1
    count_sp = lax.axis_size("sp")
    count_dp = lax.axis_size("dp")
    scale = 1.0 / math.sqrt(length * count_sp * count_dp)
    prior_value, prior_gate = from_behind(
        (value_rows[length - halo_rows :], gate_rows[length - halo_rows :]), "sp", 1
    )
    value_ext = jnp.concatenate([prior_value, value_rows], axis=0).astype(jnp.float32)
    gate_ext = jnp.concatenate([prior_gate, gate_rows], axis=0).astype(jnp.float32)
    gated_ext = value_ext * jax.nn.sigmoid(gate_ext)
    conv_rows = jnp.zeros((length, channels), jnp.float32)
    for offset in range(tap_count):
        conv_rows = conv_rows + conv_weight[offset] * gated_ext[offset : offset + length]
    centred = conv_rows - jnp.mean(conv_rows, axis=-1, keepdims=True)
    inv_std = lax.rsqrt(jnp.mean(centred * centred, axis=-1, keepdims=True) + epsilon)
    normed = centred * inv_std
    pre_act = normed * norm_gain + norm_shift
    sigmoid_pre = jax.nn.sigmoid(pre_act)
    act_rows = (pre_act * sigmoid_pre).astype(jnp.bfloat16)
    columns = cotan_rows
    grad_act = jnp.dot(
        columns,
        lax.all_gather(out_weight, "dp", axis=0, tiled=True),
        preferred_element_type=jnp.float32,
    )
    grad_pre = grad_act * sigmoid_pre * (1.0 + pre_act * (1.0 - sigmoid_pre))
    grad_normed = grad_pre * norm_gain
    grad_conv_rows = inv_std * (
        grad_normed
        - jnp.mean(grad_normed, axis=-1, keepdims=True)
        - normed * jnp.mean(grad_normed * normed, axis=-1, keepdims=True)
    )
    later_grads = from_behind(grad_conv_rows[:halo_rows], "sp", -1)
    padded_grad = jnp.concatenate([grad_conv_rows, later_grads], axis=0)
    grad_gated = jnp.zeros((length, channels), jnp.float32)
    for offset in range(tap_count):
        start = tap_count - 1 - offset
        grad_gated = grad_gated + conv_weight[offset] * padded_grad[start : start + length]
    grad_taps = jnp.stack(
        [
            jnp.sum(grad_conv_rows * gated_ext[offset : offset + length], axis=0)
            for offset in range(tap_count)
        ],
        axis=0,
    )
    sigmoid_gate = jax.nn.sigmoid(gate_ext[halo_rows:])
    grad_value = (grad_gated * sigmoid_gate).astype(jnp.bfloat16)
    grad_gate = (grad_gated * value_ext[halo_rows:] * sigmoid_gate * (1.0 - sigmoid_gate)).astype(
        jnp.bfloat16
    )
    grad_conv, grad_gain, grad_shift = lax.psum(
        (
            grad_taps * scale,
            jnp.sum(grad_pre * normed, axis=0) * scale,
            jnp.sum(grad_pre, axis=0) * scale,
        ),
        ("sp", "dp"),
    )
    columns = cotan_rows
    product = lax.dot_general(
        columns, act_rows, (((0,), (0,)), ((), ())), preferred_element_type=jnp.float32
    )
    partial_rows = lax.psum_scatter(product * scale, "dp", scatter_dimension=0, tiled=True)
    grad_out_weight = lax.psum(partial_rows, "sp")
    return (grad_value[None], grad_gate[None], grad_out_weight, grad_conv, grad_gain, grad_shift)


def solution(mesh):
    in_specs = (
        P("dp", "sp", None),
        P("dp", "sp", None),
        P("dp", "sp", None),
        P(),
        P(),
        P(),
        P("dp", None),
    )
    out_specs = (P("dp", "sp", None), P("dp", "sp", None), P("dp", None), P(), P(), P())
    return jax.shard_map(
        per_device, mesh=mesh, in_specs=in_specs, out_specs=out_specs, check_vma=False
    )
```

profile of v0, /device:TPU:0, one launch (start us, length us, event | category | flops | bytes accessed | tf_op | source)
XLA Modules:
  0.0 314.7 jit_solution(10922288983692130966)
XLA Ops:
  7.2 0.7 all-gather.2.cloned.1.call-update
  7.9 0.0 reduce-scatter.2.cloned.1.call-start
  8.0 0.8 slice_bitcast_fusion
  8.7 4.9 %collective-permute-start.1 = (bf16[30,512]{1,0:T(8,128)(2,1)S(1)}, bf16[30,512]{1,0:T(8,128)(2,1)S(1)}, u32[]{:S(2)}, u32[]{:S(2)}) collective-permute-start(bf16[30,512]{1,0:T(8,128)(2,1)S(1)} %slice_bitcast_fusion), channel_id=1, source_target_pairs={{0,2},{2,4},{4,6},{6,8},{8,10},{10,12},{12,14},{14,16},{16,18},{18... | collective-permute-start | bytes 92168 | tf_op jit(solution)/shard_map/ppermute | solution.py:14
  13.6 0.8 slice_bitcast_fusion.1
  14.4 3.4 %collective-permute-start = (bf16[30,512]{1,0:T(8,128)(2,1)S(1)}, bf16[30,512]{1,0:T(8,128)(2,1)S(1)}, u32[]{:S(2)}, u32[]{:S(2)}) collective-permute-start(bf16[30,512]{1,0:T(8,128)(2,1)S(1)} %slice_bitcast_fusion.1), channel_id=1, source_target_pairs={{0,2},{2,4},{4,6},{6,8},{8,10},{10,12},{12,14},{14,16},{16,18},{18... | collective-permute-start | bytes 92168 | tf_op jit(solution)/shard_map/ppermute | solution.py:14
  17.9 1.5 collective-permute-done
  19.4 1.7 divide_multiply_fusion
  21.1 5.0 %fusion.113 = (f32[512]{0:T(512)S(1)}, f32[512,512]{1,0:T(8,128)S(1)}) fusion(f32[542,512]{1,0:T(8,128)S(1)} %divide_multiply_fusion, f32[512]{0:T(512)S(1)} %bitcast.148, f32[512]{0:T(512)S(1)} %bitcast.150, f32[512]{0:T(512)S(1)} %bitcast.92, f32[512]{0:T(512)S(1)} %bitcast.94, f32[512]{0:T(512)S(1)} %bitcast.96, f32[512]{0:T(512)S(1)} %bitcast.98, ...), kind=kLoop, calls=%fused_computation.212 | loop fusion | flops 16252416 | bytes 33619968 | tf_op jit(solution)/shard_map/reduce_sum | solution.py:37
  26.1 0.3 multiply_reduce_fusion.33
  26.4 0.7 copy-done.2
  27.1 3.4 %multiply_bitcast_fusion = f32[2048,512]{0,1:T(8,128)} fusion(bf16[1,512,2048]{2,1,0:T(8,128)(2,1)S(1)} %copy-done, f32[512,512]{1,0:T(8,128)S(1)} %get-tuple-element.54, f32[512]{0:T(512)S(1)} %copy-done.7, f32[512]{0:T(512)S(1)} %copy-done.6, f32[512]{0:T(512)S(1)} %add_rsqrt_fusion, f32[512]{0:T(512)S(1)} %broadcast_multiply_fusion.5), kind=kOutput, calls=%fused_computation.29 | convolution fusion | flops 1077149696 | bytes 7348224 | tf_op jit(solution)/shard_map/dot_general | solution.py:83
  30.5 0.0 all-reduce.4.cloned.1.call-start
  30.5 2.4 maximum_convert_fusion.1
  32.9 1.2 maximum_convert_fusion
  34.1 5.1 %multiply_reduce_fusion = (f32[512]{0:T(512)}, f32[512]{0:T(512)S(1)}, f32[512]{0:T(512)S(1)}, f32[512]{0:T(512)}, f32[512,512]{1,0:T(8,128)}) fusion(f32[512,512]{1,0:T(8,128)} %copy-done.2, f32[512]{0:T(512)S(1)} %add_rsqrt_fusion, f32[512]{0:T(512)S(1)} %broadcast_multiply_fusion.5, f32[512]{0:T(512)S(1)} %copy-done.6, f32[512]{0:T(512)S(1)} %copy-done.7, ...), kind=kOutput, calls=%fused_computation.151 | convolution fusion | flops 1078720512 | bytes 6307840 | tf_op jit(solution)/shard_map/dot_general | solution.py:44
  39.2 5.3 %reduce-scatter.2.cloned.1.call-done = f32[1024,512]{0,1:T(8,128)} async-done(((f32[2048,512]{0,1:T(8,128)}), f32[1024,512]{0,1:T(8,128)}) %reduce-scatter.2.cloned.1.call-update) | async-done | bytes 2097168 | tf_op jit(solution)/shard_map/reduce_scatter | solution.py:86
  44.5 0.0 all-reduce.6.cloned.1.call-start
  44.6 4.2 %multiply_reduce_fusion.1 = (f32[512]{0:T(512)S(1)}, f32[512]{0:T(512)S(1)}, f32[512]{0:T(512)S(1)}, f32[512]{0:T(512)S(1)}, f32[512]{0:T(512)S(1)}, /*index=5*/...) fusion(f32[542,512]{1,0:T(8,128)S(1)} %divide_multiply_fusion, ...), kind=kLoop, calls=%fused_computation.152 | loop fusion | flops 11262976 | bytes 22067200 | tf_op jit(solution)/shard_map/reduce_sum | solution.py:64
  48.8 1.5 collective-permute-start.2
  50.3 2.3 multiply_reduce_fusion.19
  52.6 1.6 stack.127
  54.2 0.6 broadcast_multiply_fusion
  54.8 1.3 broadcast_multiply_fusion.1
  56.1 23.0 %fusion.105 = (bf16[1,512,512]{2,1,0:T(8,128)(2,1)}, f32[512,512]{1,0:T(8,128)S(1)}) fusion(f32[542,512]{1,0:T(8,128)} %maximum_convert_fusion, f32[542,512]{1,0:T(8,128)} %maximum_convert_fusion.1, f32[512,512]{1,0:T(8,128)} %copy-done.1, f32[512]{0:T(512)S(1)} %bitcast.149, f32[30,512]{1,0:T(8,128)S(1)} %collective-permute-done.2, f32[512]{0:T(512)S(1)} %bitcast.151, ...), kind=kLoop, calls=%fused_computation.196 | loop fusion | flops 25952256 | bytes 4843520 | tf_op jit(solution)/shard_map/broadcast_in_dim | solution.py:88
  79.2 1.1 fusion.104
  80.2 97.6 %all-reduce.4.cloned.1.call-done = f32[1024,512]{0,1:T(8,128)} async-done(((f32[1024,512]{0,1:T(8,128)}), f32[1024,512]{0,1:T(8,128)}) %all-reduce.4.cloned.1.call-update) | async-done | bytes 2097168 | tf_op jit(solution)/shard_map/psum | solution.py:87
  177.9 2.9 copy.13
  180.7 123.4 %all-reduce.6.cloned.1.call-done = (f32[31,512]{1,0:T(8,128)}, f32[512]{0:T(512)}, f32[512]{0:T(512)}) async-done(((f32[31,512]{1,0:T(8,128)}, f32[512]{0:T(512)}, f32[512]{0:T(512)}), (f32[31,512]{1,0:T(8,128)}, f32[512]{0:T(512)}, f32[512]{0:T(512)})) %all-reduce.6.cloned.1.call-update) | async-done | bytes 67600 | tf_op jit(solution)/shard_map/psum | solution.py:74
  304.2 1.5 copy.18
  305.6 1.3 copy.19
  306.9 1.2 copy.20
  (28 shorter events, 0.2 us)
Async XLA Ops:
  7.2 19.9 %copy-start = (bf16[1,512,2048]{2,1,0:T(8,128)(2,1)S(1)}, bf16[1,512,2048]{2,1,0:T(8,128)(2,1)}, u32[]{:S(2)}) copy-start(bf16[1,512,2048]{2,1,0:T(8,128)(2,1)} %param.9) | copy-start | bytes 6291460
  7.2 10.6 %copy-start.5 = (f32[31,512]{1,0:T(8,128)S(1)}, f32[31,512]{1,0:T(8,128)}, u32[]{:S(2)}) copy-start(f32[31,512]{1,0:T(8,128)} %param.10) | copy-start | bytes 190468
  7.2 26.9 %all-gather.2.cloned.1.call-start = ((), (), s32[]{:S(2)}) async-start(), calls=%async_computation.1 | async-start | bytes 3145728 | tf_op jit(solution)/shard_map/all_gather | solution.py:46
  7.9 36.6 %reduce-scatter.2.cloned.1.call-start = ((), (), s32[]{:S(2)}) async-start(), calls=%async_computation.2 | async-start | bytes 6291456 | tf_op jit(solution)/shard_map/reduce_scatter | solution.py:86
  8.7 9.1 %collective-permute-start.1 = (bf16[30,512]{1,0:T(8,128)(2,1)S(1)}, bf16[30,512]{1,0:T(8,128)(2,1)S(1)}, u32[]{:S(2)}, u32[]{:S(2)}) collective-permute-start(bf16[30,512]{1,0:T(8,128)(2,1)S(1)} %slice_bitcast_fusion), channel_id=1, source_target_pairs={{0,2},{2,4},{4,6},{6,8},{8,10},{10,12},{12,14},{14,16},{16,18},{18... | collective-permute-start | bytes 92168 | tf_op jit(solution)/shard_map/ppermute | solution.py:14
  14.4 5.0 %collective-permute-start = (bf16[30,512]{1,0:T(8,128)(2,1)S(1)}, bf16[30,512]{1,0:T(8,128)(2,1)S(1)}, u32[]{:S(2)}, u32[]{:S(2)}) collective-permute-start(bf16[30,512]{1,0:T(8,128)(2,1)S(1)} %slice_bitcast_fusion.1), channel_id=1, source_target_pairs={{0,2},{2,4},{4,6},{6,8},{8,10},{10,12},{12,14},{14,16},{16,18},{18... | collective-permute-start | bytes 92168 | tf_op jit(solution)/shard_map/ppermute | solution.py:14
  21.1 6.0 %copy-start.6 = (f32[512]{0:T(512)S(1)}, f32[512]{0:T(512)}, u32[]{:S(2)}) copy-start(f32[512]{0:T(512)} %param.11) | copy-start | bytes 6148
  21.1 6.0 %copy-start.7 = (f32[512]{0:T(512)S(1)}, f32[512]{0:T(512)}, u32[]{:S(2)}) copy-start(f32[512]{0:T(512)} %param.12) | copy-start | bytes 6148
  26.1 1.0 copy-start.2
  30.5 147.4 %all-reduce.4.cloned.1.call-start = ((), (), s32[]{:S(2)}) async-start(), calls=%async_computation.3 | async-start | bytes 4194304 | tf_op jit(solution)/shard_map/psum | solution.py:87
  30.5 2.4 copy-start.4
  44.5 259.6 %all-reduce.6.cloned.1.call-start = ((), (), s32[]{:S(2)}) async-start(), calls=%async_computation.4 | async-start | bytes 139264 | tf_op jit(solution)/shard_map/psum | solution.py:74
  48.8 3.8 %copy-start.1 = (f32[512,512]{1,0:T(8,128)}, f32[512,512]{1,0:T(8,128)S(1)}, u32[]{:S(2)}) copy-start(f32[512,512]{1,0:T(8,128)S(1)} %get-tuple-element.50) | copy-start | bytes 3145732
  48.8 7.3 %collective-permute-start.2 = (f32[30,512]{1,0:T(8,128)S(1)}, f32[30,512]{1,0:T(8,128)S(1)}, u32[]{:S(2)}, u32[]{:S(2)}) collective-permute-start(f32[30,512]{1,0:T(8,128)S(1)} %slice.489), channel_id=1, source_target_pairs={{2,0},{4,2},{6,4},{8,6},{10,8},{12,10},{14,12},{16,14},{18,16},{20... | collective-permute-start | bytes 184328 | tf_op jit(solution)/shard_map/ppermute | solution.py:14
  56.1 23.1 %copy-start.3 = (f32[542,512]{1,0:T(8,128)S(1)}, f32[542,512]{1,0:T(8,128)}, u32[]{:S(2)}) copy-start(f32[542,512]{1,0:T(8,128)} %maximum_convert_fusion.1) | copy-start | bytes 3330052
Sparse Core Ops, SparseCore 0:
  9.5 13.2 all-gather.1
  30.6 13.8 reduce-scatter.1
  50.0 127.8 all-reduce.3
  184.2 119.8 all-reduce.5
where the time goes:
time: 317 us; the launch traced here: 315 us
  waiting for transfers between devices  229 us (72%)
  other arithmetic  43 us (14%)
  between operations  14 us (4%)
  local copies, waits for them, and re-layouts  10.7 us (3%)
  starting transfers between devices  9.9 us (3%)
  matrix products  8.5 us (3%)
    psum x1, waiting for transfers between devices, per_device(): lax.psum((grad_taps * scale, jnp.sum(grad_pre * normed, axis=0) * scale,...  123 us
    psum x1, waiting for transfers between devices, per_device(): grad_out_weight = lax.psum(partial_rows, 'sp')  97.6 us
    broadcast_in_dim x1, other arithmetic, per_device(): grad_gate[None]  23 us
    ppermute x3, starting transfers between devices, from_behind(): return lax.ppermute(value, axis, pairs)  9.74 us
    unnamed x20, local copies, waits for them, and re-layouts  7.56 us
    reduce_sum x2, other arithmetic, per_device(): jnp.sum(grad_conv_rows * gated_ext[offset:offset + length], axis=0)  6.52 us
  transfers between devices with their start and end apart: 7, of which 4 were waited for; matrix products, arithmetic and copies ran while one was open for 18% of the time, Pallas kernels for 0%

commit v1 on v0

v1 whole, which is shorter than its diff:
```python
import functools
import math

import jax
import jax.numpy as jnp
from jax import lax
from jax.experimental import pallas as pl
from jax.experimental.pallas import tpu as pltpu
from jax.sharding import PartitionSpec as P

epsilon = 1e-06
LANES = 128
STREAMS = 4
NARROW_STAGES = 2
MAX_HALVINGS = 3
f32 = jnp.float32
bf16 = jnp.bfloat16


def flip(index, bit):
    size = 1 << bit
    here = (index // size) % 2
    return here, index + (1 - 2 * here) * size


def stage_plan(n_sp, rows):
    bits = int(math.log2(n_sp))
    plan = []
    for stage in range(bits):
        halve = stage < MAX_HALVINGS and rows // 2 >= 16
        plan.append((halve, rows))
        if halve:
            rows //= 2
    return plan, rows


def bit_order(n_sp, stream):
    order = list(range(int(math.log2(n_sp))))
    if stream % 2 and len(order) > 1:
        order[0], order[1] = order[1], order[0]
    return order


def kernel(
    n_sp, n_dp, plan,
    value, gate, cotan, taps, gain, shift, weight,
    grad_value, grad_gate, out_weight, out_small,
    gated, grads, normed, inv, act, grad_act, weights,
    halo_v, halo_g, edge_out, edge_in, sums, small, small_in,
    dp_out, dp_in, acc, narrow_out, narrow_in, wide_in, full_in, gathered,
    local_sem, w_send, w_recv, h_send, h_recv, dp_send, dp_recv, st_send, st_recv, sm_send, sm_recv,
):
    sp = lax.axis_index("sp")
    dp = lax.axis_index("dp")
    length, channels = value.shape
    tap_count = taps.shape[0]
    blocks = channels // LANES
    ext = grads.shape[1] - length
    lead = ext - (tap_count - 1)
    local_rows = weight.shape[0]
    streams, stream_rows = acc.shape[0], acc.shape[1]
    block_rows = min(64, length)
    row_blocks = length // block_rows
    sp_bits = int(math.log2(n_sp))
    dp_bits = int(math.log2(n_dp))
    later = (sp + 1) % n_sp
    prior = (sp + n_sp - 1) % n_sp

    barrier = pltpu.get_barrier_semaphore()
    partners = [{"sp": later}, {"sp": prior}]
    partners += [{"sp": flip(sp, b)[1]} for b in range(sp_bits)]
    partners += [{"dp": (dp + o) % n_dp} for o in range(1, n_dp)]
    for partner in partners:
        pl.semaphore_signal(barrier, inc=1, device_id=partner, device_id_type=pl.DeviceIdType.MESH)
    pl.semaphore_wait(barrier, len(partners))

    def remote(src, dst, send, recv, where):
        return pltpu.make_async_remote_copy(
            src_ref=src, dst_ref=dst, send_sem=send, recv_sem=recv,
            device_id=where, device_id_type=pl.DeviceIdType.MESH,
        )

    halos = [
        remote(value.at[pl.ds(length - ext, ext)], halo_v, h_send.at[0], h_recv.at[0], {"sp": later}),
        remote(gate.at[pl.ds(length - ext, ext)], halo_g, h_send.at[1], h_recv.at[1], {"sp": later}),
    ]
    for copy in halos:
        copy.start()
    own = pltpu.make_async_copy(weight, weights.at[dp], local_sem)
    own.start()
    w_copies = []
    for o in range(1, n_dp):
        w_copies.append(
            remote(weight, weights.at[dp], w_send.at[o - 1], w_recv.at[o - 1], {"dp": (dp + o) % n_dp})
        )
        w_copies[-1].start()

    def cols(b):
        return pl.ds(b * LANES, LANES)

    def gate_rows(v, g):
        return v.astype(f32) * jax.nn.sigmoid(g.astype(f32))

    def gating(i, _):
        r0 = pl.multiple_of(i * block_rows, block_rows)
        for b in range(blocks):
            gated[b, pl.ds(ext + r0, block_rows), :] = gate_rows(
                value[pl.ds(r0, block_rows), cols(b)], gate[pl.ds(r0, block_rows), cols(b)]
            )
        return 0

    lax.fori_loop(0, row_blocks, gating, 0)
    for copy in halos:
        copy.wait()
    for b in range(blocks):
        gated[b, 0:ext, :] = jnp.where(sp > 0, gate_rows(halo_v[:, cols(b)], halo_g[:, cols(b)]), 0.0)

    def row_mean(parts):
        total = parts[0]
        for p in parts[1:]:
            total = total + p
        return jnp.sum(total, axis=-1, keepdims=True) * (1.0 / channels)

    def forward(i, _):
        r0 = pl.multiple_of(i * block_rows, block_rows)
        rows = pl.ds(r0, block_rows)
        convs = []
        for b in range(blocks):
            total = jnp.zeros((block_rows, LANES), f32)
            for j in range(tap_count):
                total = total + taps[j : j + 1, cols(b)] * gated[b, pl.ds(r0 + lead + j, block_rows), :]
            convs.append(total)
        mean = row_mean(convs)
        centred = [c - mean for c in convs]
        inv_std = lax.rsqrt(row_mean([c * c for c in centred]) + epsilon)
        inv[rows, :] = inv_std
        for b in range(blocks):
            n = centred[b] * inv_std
            normed[rows, cols(b)] = n
            pre = n * gain[:, cols(b)] + shift[:, cols(b)]
            act[rows, cols(b)] = (pre * jax.nn.sigmoid(pre)).astype(bf16)
        return 0

    lax.fori_loop(0, row_blocks, forward, 0)

    dp_copies = [[None] * (n_dp - 1) for _ in range(streams)]

    def product(chunk, stream):
        start = pl.multiple_of(chunk * local_rows + stream * stream_rows, LANES)
        return lax.dot_general(
            cotan[:, pl.ds(start, stream_rows)], act[...], (((0,), (0,)), ((), ())),
            preferred_element_type=f32,
        )

    for k in range(streams):
        for o in range(1, n_dp):
            peer = (dp + o) % n_dp
            dp_out[o - 1, k] = product(peer, k)
            copy = remote(
                dp_out.at[o - 1, k], dp_in.at[o - 1, k],
                dp_send.at[k, o - 1], dp_recv.at[k, o - 1], {"dp": peer},
            )
            copy.start()
            dp_copies[k][o - 1] = copy
        acc[k] = product(dp, k)

    def exchange(k):
        order = bit_order(n_sp, k)
        for copy in dp_copies[k]:
            copy.wait()
        for o in range(1, n_dp):
            acc[k] += dp_in[o - 1, k]
        off = 0
        final = stream_rows
        for stage, (halve, rows) in enumerate(plan):
            here, partner = flip(sp, order[stage])
            sems = st_send.at[k, stage], st_recv.at[k, stage], {"sp": partner}
            if halve:
                half = rows // 2
                final = half
                spot = pl.ds(stream_rows - rows, half)
                out = pl.ds(pl.multiple_of(off + (1 - here) * half, half), half)
                off = off + here * half
                into = pl.ds(pl.multiple_of(off, half), half)
                if stage < NARROW_STAGES:
                    narrow_out[k, spot, :] = acc[k, out, :].astype(bf16)
                    copy = remote(narrow_out.at[k, spot], narrow_in.at[k, spot], *sems)
                    landed = narrow_in
                else:
                    copy = remote(acc.at[k, out], wide_in.at[k, spot], *sems)
                    landed = wide_in
                copy.start()
                yield
                copy.wait()
                acc[k, into, :] += landed[k, spot, :].astype(f32)
            else:
                into = pl.ds(pl.multiple_of(off, rows), rows)
                copy = remote(acc.at[k, into], full_in.at[k, stage], *sems)
                copy.start()
                yield
                copy.wait()
                acc[k, into, :] += full_in[k, stage]
        spot = pl.ds(pl.multiple_of(off, final), final)
        wide = pl.ds(pl.multiple_of(k * stream_rows + off, final), final)
        gathered[wide, :] = acc[k, spot, :].astype(bf16)
        for stage in reversed(range(len(plan))):
            halve, rows = plan[stage]
            if not halve:
                continue
            half = rows // 2
            here, partner = flip(sp, order[stage])
            spot = pl.ds(pl.multiple_of(k * stream_rows + off, half), half)
            back = len(plan) + stage
            copy = remote(
                gathered.at[spot], gathered.at[spot],
                st_send.at[k, back], st_recv.at[k, back], {"sp": partner},
            )
            copy.start()
            yield
            copy.wait()
            off = off - here * half
        out_weight[pl.ds(k * stream_rows, stream_rows), :] = gathered[pl.ds(k * stream_rows, stream_rows), :]

    def combine():
        step = 0
        axes = [("dp", dp, b) for b in range(dp_bits)] + [("sp", sp, b) for b in range(sp_bits)]
        for name, index, b in axes:
            copy = remote(small, small_in.at[step], sm_send.at[step], sm_recv.at[step], {name: flip(index, b)[1]})
            copy.start()
            yield
            copy.wait()
            small[...] += small_in[step]
            step += 1
        out_small[...] = small[...]

    flows = [exchange(k) for k in range(streams)]

    def advance():
        for flow in list(flows):
            if next(flow, "end") == "end":
                flows.remove(flow)

    for copy in w_copies:
        copy.wait()
    own.wait()
    total = None
    for d in range(n_dp):
        part = jnp.dot(cotan[:, d * local_rows : (d + 1) * local_rows], weights[d], preferred_element_type=f32)
        total = part if total is None else total + part
    grad_act[...] = total
    advance()
    sums[...] = jnp.zeros_like(sums)

    def backward(i):
        r0 = pl.multiple_of(i * block_rows, block_rows)
        rows = pl.ds(r0, block_rows)
        inv_std = inv[rows, :]
        normal, grad_normal = [], []
        for b in range(blocks):
            n = normed[rows, cols(b)]
            pre = n * gain[:, cols(b)] + shift[:, cols(b)]
            s = jax.nn.sigmoid(pre)
            grad_pre = grad_act[rows, cols(b)] * s * (1.0 + pre * (1.0 - s))
            sums[0, b] += jnp.sum((grad_pre * n).reshape(block_rows // 8, 8, LANES), axis=0)
            sums[1, b] += jnp.sum(grad_pre.reshape(block_rows // 8, 8, LANES), axis=0)
            normal.append(n)
            grad_normal.append(grad_pre * gain[:, cols(b)])
        first = row_mean(grad_normal)
        second = row_mean([g * n for g, n in zip(grad_normal, normal)])
        for b in range(blocks):
            grads[b, rows, :] = inv_std * (grad_normal[b] - first - normal[b] * second)

    backward(0)
    edge_out[...] = grads[:, 0:ext, :]
    edge = remote(edge_out, edge_in, h_send.at[2], h_recv.at[2], {"sp": prior})
    edge.start()

    def backward_loop(i, _):
        backward(i)
        return 0

    lax.fori_loop(1, row_blocks, backward_loop, 0)
    advance()

    small[...] = jnp.zeros_like(small)
    for b in range(blocks):

        def tap_rows(i, carry):
            r0 = pl.multiple_of(i * 8, 8)
            g = grads[b, pl.ds(r0, 8), :]
            return tuple(c + g * gated[b, pl.ds(r0 + lead + j, 8), :] for j, c in enumerate(carry))

        found = lax.fori_loop(
            0, length // 8, tap_rows, tuple(jnp.zeros((8, LANES), f32) for _ in range(tap_count))
        )
        for j in range(tap_count):
            small[j : j + 1, cols(b)] = jnp.sum(found[j], axis=0, keepdims=True)
        for row in range(2):
            small[tap_count + row : tap_count + row + 1, cols(b)] = jnp.sum(sums[row, b], axis=0, keepdims=True)
        if b % 2:
            advance()
    flows.insert(0, combine())
    edge.wait()
    for b in range(blocks):
        grads[b, pl.ds(length, ext), :] = jnp.where(sp < n_sp - 1, edge_in[b], 0.0)
    advance()

    def final_rows(i, _):
        r0 = pl.multiple_of(i * block_rows, block_rows)
        rows = pl.ds(r0, block_rows)
        for b in range(blocks):
            total = jnp.zeros((block_rows, LANES), f32)
            for j in range(tap_count):
                total = total + taps[j : j + 1, cols(b)] * grads[b, pl.ds(r0 + tap_count - 1 - j, block_rows), :]
            s = jax.nn.sigmoid(gate[rows, cols(b)].astype(f32))
            grad_value[rows, cols(b)] = (total * s).astype(bf16)
            grad_gate[rows, cols(b)] = (total * value[rows, cols(b)].astype(f32) * s * (1.0 - s)).astype(bf16)
        return 0

    pieces = math.gcd(row_blocks, 4)
    step = row_blocks // pieces
    for piece in range(pieces):
        lax.fori_loop(piece * step, (piece + 1) * step, final_rows, 0)
        advance()
    while flows:
        advance()


def per_device(glu_value, glu_gate, cotangent, conv_weight, norm_gain, norm_shift, out_weight):
    n_sp, n_dp = lax.axis_size("sp"), lax.axis_size("dp")
    length, channels = glu_value.shape[1:]
    features = cotangent.shape[2]
    tap_count = conv_weight.shape[0]
    local_rows = out_weight.shape[0]
    scale = 1.0 / math.sqrt(length * n_sp * n_dp)
    ext = -(-(tap_count - 1) // 16) * 16
    blocks = channels // LANES
    streams = STREAMS
    while streams > 1 and (local_rows // streams) % LANES:
        streams //= 2
    stream_rows = local_rows // streams
    plan, final = stage_plan(n_sp, stream_rows)
    full_rows = max([rows for halve, rows in plan if not halve] + [8])
    small_rows = -(-(tap_count + 2) // 8) * 8
    steps = int(math.log2(n_sp)) + int(math.log2(n_dp))
    dma = pltpu.SemaphoreType.DMA
    vmem = pltpu.VMEM
    peers = max(n_dp - 1, 1)
    spec = pl.BlockSpec(memory_space=pltpu.VMEM)
    grad_value, grad_gate, grad_weight, small = pl.pallas_call(
        functools.partial(kernel, n_sp, n_dp, plan),
        out_shape=[
            jax.ShapeDtypeStruct((length, channels), bf16),
            jax.ShapeDtypeStruct((length, channels), bf16),
            jax.ShapeDtypeStruct((local_rows, channels), bf16),
            jax.ShapeDtypeStruct((small_rows, channels), f32),
        ],
        in_specs=[spec] * 7,
        out_specs=[spec] * 4,
        scratch_shapes=[
            vmem((blocks, ext + length, LANES), f32),
            vmem((blocks, length + ext, LANES), f32),
            vmem((length, channels), f32),
            vmem((length, 1), f32),
            vmem((length, channels), bf16),
            vmem((length, channels), f32),
            vmem((n_dp, local_rows, channels), bf16),
            vmem((ext, channels), bf16),
            vmem((ext, channels), bf16),
            vmem((blocks, ext, LANES), f32),
            vmem((blocks, ext, LANES), f32),
            vmem((2, blocks, 8, LANES), f32),
            vmem((small_rows, channels), f32),
            vmem((steps, small_rows, channels), f32),
            vmem((peers, streams, stream_rows, channels), f32),
            vmem((peers, streams, stream_rows, channels), f32),
            vmem((streams, stream_rows, channels), f32),
            vmem((streams, stream_rows, channels), bf16),
            vmem((streams, stream_rows, channels), bf16),
            vmem((streams, stream_rows, channels), f32),
            vmem((streams, len(plan), full_rows, channels), f32),
            vmem((local_rows, channels), bf16),
            dma,
            dma((peers,)), dma((peers,)),
            dma((3,)), dma((3,)),
            dma((streams, peers)), dma((streams, peers)),
            dma((streams, 2 * len(plan))), dma((streams, 2 * len(plan))),
            dma((steps,)), dma((steps,)),
        ],
        compiler_params=pltpu.CompilerParams(
            collective_id=0, has_side_effects=True, vmem_limit_bytes=60 * 1024 * 1024
        ),
    )(glu_value[0], glu_gate[0], cotangent[0], conv_weight, norm_gain[None], norm_shift[None], out_weight)
    small = small * scale
    return (
        grad_value[None],
        grad_gate[None],
        grad_weight.astype(f32) * scale,
        small[:tap_count],
        small[tap_count],
        small[tap_count + 1],
    )


def solution(mesh):
    in_specs = (
        P("dp", "sp", None),
        P("dp", "sp", None),
        P("dp", "sp", None),
        P(),
        P(),
        P(),
        P("dp", None),
    )
    out_specs = (P("dp", "sp", None), P("dp", "sp", None), P("dp", None), P(), P(), P())
    return jax.shard_map(
        per_device, mesh=mesh, in_specs=in_specs, out_specs=out_specs, check_vma=False
    )
```

time: 317 us -> 72.8 us (0.23)
  waiting for transfers between devices: 229 us -> 0 us
  Pallas kernels: 0 us -> 65.3 us
  other arithmetic: 43 us -> 3.85 us
  between operations: 14 us -> 0.65 us
  starting transfers between devices: 9.9 us -> 0 us
  matrix products: 8.5 us -> 0 us
  local copies, waits for them, and re-layouts: 10.7 us -> 2.82 us
    psum x2 -> x0, waiting for transfers between devices: 221 us -> none  [the longest x1 123 us: per_device(): lax.psum((grad_taps * scale, jnp.sum(grad_pre * normed, axis=0) * scale,...]
    pallas_call x0 -> x1, Pallas kernels: none -> 65.3 us  [per_device(): pl.pallas_call(functools.partial(kernel, n_sp, n_dp, plan), out_shape=[ja...]
    broadcast_in_dim x2 -> x0, other arithmetic: 24.1 us -> none  [the longest x1 23 us: per_device(): grad_gate[None]]
    reduce_sum x4 -> x0, other arithmetic: 11.8 us -> none  [the longest x2 6.52 us: per_device(): jnp.sum(grad_conv_rows * gated_ext[offset:offset + length], axis=0)]
    ppermute x3 -> x0, starting transfers between devices: 9.74 us -> none  [from_behind(): return lax.ppermute(value, axis, pairs)]
    dot_general x2 -> x0, matrix products: 8.5 us -> none  [the longest x1 5.1 us: per_device(): jnp.dot(columns, lax.all_gather(out_weight, 'dp', axis=0, tiled=True), pr...]
    unnamed x20 -> x6, local copies, waits for them, and re-layouts: 7.56 us -> 1.59 us
    reduce_scatter x1 -> x0, waiting for transfers between devices: 5.34 us -> none  [per_device(): lax.psum_scatter(product * scale, 'dp', scatter_dimension=0, tiled=True)]
  transfers between devices with their start and end apart: 7 -> 0, of which waited for: 4 -> 0; matrix products, arithmetic and copies ran while one was open for 18% -> 0% of each run, Pallas kernels for 0% -> 0%
where the time goes in v1:
time: 72.8 us; the launch traced here: 72.6 us
  Pallas kernels  65.3 us (90%)
  other arithmetic  3.85 us (5%)
  local copies, waits for them, and re-layouts  2.82 us (4%)
    pallas_call x1, Pallas kernels, per_device(): pl.pallas_call(functools.partial(kernel, n_sp, n_dp, plan), out_shape=[ja...  65.3 us
    mul x1, other arithmetic, per_device(): grad_weight.astype(f32) * scale  2.89 us
    unnamed x6, local copies, waits for them, and re-layouts  1.59 us

profile of v1, /device:TPU:0, one launch (start us, length us, event | category | flops | bytes accessed | tf_op | source)
XLA Modules:
  0.0 72.6 jit_solution(2558396474700606185)
XLA Ops:
  0.6 65.3 %shard_map.118 = (bf16[512,512]{1,0:T(8,128)(2,1)}, bf16[512,512]{1,0:T(8,128)(2,1)}, bf16[1024,512]{1,0:T(8,128)(2,1)}, f32[40,512]{1,0:T(8,128)}) custom-call(bf16[512,512]{1,0:T(8,128)(2,1)} %bitcast.10, bf16[512,512]{1,0:T(8,128)(2,1)} %bitcast.11, bf16[512,2048]{1,0:T(8,128)(2,1)} %bitcast.9, f32[31,512]{1,0:T(8,128)} %taps.1, f32[1,512]{1,0:T(1,128)} %bitcast.14, ...), custom_call_target="tpu_custom_call" | custom-call | tf_op jit(solution)/shard_map/pallas_call | solution.py:350
  65.9 0.0 copy-start.1
  66.0 1.0 %broadcast_multiply_fusion = f32[40,512]{1,0:T(8,128)S(1)} fusion(f32[40,512]{1,0:T(8,128)} %get-tuple-element.13), kind=kLoop, calls=%fused_computation.1 | loop fusion | flops 20480 | bytes 163840 | tf_op jit(solution)/shard_map/mul | solution.py:394
  66.9 0.6 fusion
  67.5 0.6 slice.12
  68.1 0.0 copy-start
  68.1 2.9 %convert_multiply_fusion = f32[1024,512]{1,0:T(8,128)} fusion(bf16[1024,512]{1,0:T(8,128)(2,1)} %get-tuple-element.12), kind=kLoop, calls=%fused_computation | loop fusion | flops 1048576 | bytes 3145728 | tf_op jit(solution)/shard_map/mul | solution.py:398
  71.0 0.0 copy-done.1
  71.0 0.8 %copy.15 = bf16[1,512,512]{2,1,0:T(8,128)(2,1)} copy(bf16[1,512,512]{2,1,0:T(8,128)(2,1)S(1)} %bitcast.13) | data formatting | bytes 1048576
  71.8 0.0 copy-done
  71.8 0.8 %copy.16 = bf16[1,512,512]{2,1,0:T(8,128)(2,1)} copy(bf16[1,512,512]{2,1,0:T(8,128)(2,1)S(1)} %bitcast.12) | data formatting | bytes 1048576
Async XLA Ops:
  65.9 5.1 %copy-start.1 = (bf16[512,512]{1,0:T(8,128)(2,1)S(1)}, bf16[512,512]{1,0:T(8,128)(2,1)}, u32[]{:S(2)}) copy-start(bf16[512,512]{1,0:T(8,128)(2,1)} %get-tuple-element.10) | copy-start | bytes 1572868
  68.1 3.7 %copy-start = (bf16[512,512]{1,0:T(8,128)(2,1)S(1)}, bf16[512,512]{1,0:T(8,128)(2,1)}, u32[]{:S(2)}) copy-start(bf16[512,512]{1,0:T(8,128)(2,1)} %get-tuple-element.11) | copy-start | bytes 1572868

commit v2 on v1

--- a/solution.py
+++ b/solution.py
@@ -11,8 +11,9 @@
 epsilon = 1e-06
 LANES = 128
 STREAMS = 4
-NARROW_STAGES = 2
-MAX_HALVINGS = 3
+NARROW_STAGES = 3
+MAX_HALVINGS = 4
+SMALL_HALVINGS = 2
 f32 = jnp.float32
 bf16 = jnp.bfloat16
 
@@ -42,11 +43,11 @@
 
 
 def kernel(
-    n_sp, n_dp, plan,
+    n_sp, n_dp, plan, scale,
     value, gate, cotan, taps, gain, shift, weight,
-    grad_value, grad_gate, out_weight, out_small,
+    grad_value, grad_gate, out_weight, out_taps, out_gain, out_shift,
     gated, grads, normed, inv, act, grad_act, weights,
-    halo_v, halo_g, edge_out, edge_in, sums, small, small_in,
+    halo_v, halo_g, edge_out, edge_in, sums, small, small_in, small_done,
     dp_out, dp_in, acc, narrow_out, narrow_in, wide_in, full_in, gathered,
     local_sem, w_send, w_recv, h_send, h_recv, dp_send, dp_recv, st_send, st_recv, sm_send, sm_recv,
 ):
@@ -110,10 +111,11 @@
         return 0
 
     lax.fori_loop(0, row_blocks, gating, 0)
-    for copy in halos:
-        copy.wait()
-    for b in range(blocks):
-        gated[b, 0:ext, :] = jnp.where(sp > 0, gate_rows(halo_v[:, cols(b)], halo_g[:, cols(b)]), 0.0)
+    def fill_halo():
+        for copy in halos:
+            copy.wait()
+        for b in range(blocks):
+            gated[b, 0:ext, :] = jnp.where(sp > 0, gate_rows(halo_v[:, cols(b)], halo_g[:, cols(b)]), 0.0)
 
     def row_mean(parts):
         total = parts[0]
@@ -141,7 +143,9 @@
             act[rows, cols(b)] = (pre * jax.nn.sigmoid(pre)).astype(bf16)
         return 0
 
-    lax.fori_loop(0, row_blocks, forward, 0)
+    lax.fori_loop(1, row_blocks, forward, 0)
+    fill_halo()
+    forward(0, 0)
 
     dp_copies = [[None] * (n_dp - 1) for _ in range(streams)]
 
@@ -151,18 +155,6 @@
             cotan[:, pl.ds(start, stream_rows)], act[...], (((0,), (0,)), ((), ())),
             preferred_element_type=f32,
         )
-
-    for k in range(streams):
-        for o in range(1, n_dp):
-            peer = (dp + o) % n_dp
-            dp_out[o - 1, k] = product(peer, k)
-            copy = remote(
-                dp_out.at[o - 1, k], dp_in.at[o - 1, k],
-                dp_send.at[k, o - 1], dp_recv.at[k, o - 1], {"dp": peer},
-            )
-            copy.start()
-            dp_copies[k][o - 1] = copy
-        acc[k] = product(dp, k)
 
     def exchange(k):
         order = bit_order(n_sp, k)
@@ -222,16 +214,37 @@
         out_weight[pl.ds(k * stream_rows, stream_rows), :] = gathered[pl.ds(k * stream_rows, stream_rows), :]
 
     def combine():
-        step = 0
         axes = [("dp", dp, b) for b in range(dp_bits)] + [("sp", sp, b) for b in range(sp_bits)]
-        for name, index, b in axes:
-            copy = remote(small, small_in.at[step], sm_send.at[step], sm_recv.at[step], {name: flip(index, b)[1]})
+        low, count = 0, blocks
+        halved = []
+        for step, (name, index, b) in enumerate(axes):
+            here, partner = flip(index, b)
+            sems = sm_send.at[step], sm_recv.at[step], {name: partner}
+            if step < SMALL_HALVINGS and count > 1:
+                count //= 2
+                src = small.at[pl.ds(low + (1 - here) * count, count)]
+                low = low + here * count
+                halved.append((here, count, name, partner))
+            else:
+                src = small.at[pl.ds(low, count)]
+            copy = remote(src, small_in.at[step, pl.ds(0, count)], *sems)
             copy.start()
             yield
             copy.wait()
-            small[...] += small_in[step]
-            step += 1
-        out_small[...] = small[...]
+            small[pl.ds(low, count)] += small_in[step, 0:count]
+        small_done[pl.ds(low, count)] = small[pl.ds(low, count)]
+        for back, (here, count, name, partner) in enumerate(reversed(halved)):
+            slot = len(axes) + back
+            span = small_done.at[pl.ds(low, count)]
+            copy = remote(span, span, sm_send.at[slot], sm_recv.at[slot], {name: partner})
+            copy.start()
+            yield
+            copy.wait()
+            low = low - here * count
+        for b in range(blocks):
+            out_taps[:, cols(b)] = small_done[b, 0:tap_count, :] * scale
+            out_gain[:, cols(b)] = small_done[b, tap_count : tap_count + 1, :] * scale
+            out_shift[:, cols(b)] = small_done[b, tap_count + 1 : tap_count + 2, :] * scale
 
     flows = [exchange(k) for k in range(streams)]
 
@@ -239,6 +252,21 @@
         for flow in list(flows):
             if next(flow, "end") == "end":
                 flows.remove(flow)
+
+    for k in range(streams):
+        for o in range(1, n_dp):
+            peer = (dp + o) % n_dp
+            dp_out[o - 1, k] = product(peer, k)
+            copy = remote(
+                dp_out.at[o - 1, k], dp_in.at[o - 1, k],
+                dp_send.at[k, o - 1], dp_recv.at[k, o - 1], {"dp": peer},
+            )
+            copy.start()
+            dp_copies[k][o - 1] = copy
+        acc[k] = product(dp, k)
+        if k:
+            next(flows[k - 1])
+    next(flows[streams - 1])
 
     for copy in w_copies:
         copy.wait()
@@ -294,9 +322,9 @@
             0, length // 8, tap_rows, tuple(jnp.zeros((8, LANES), f32) for _ in range(tap_count))
         )
         for j in range(tap_count):
-            small[j : j + 1, cols(b)] = jnp.sum(found[j], axis=0, keepdims=True)
+            small[b, j : j + 1, :] = jnp.sum(found[j], axis=0, keepdims=True)
         for row in range(2):
-            small[tap_count + row : tap_count + row + 1, cols(b)] = jnp.sum(sums[row, b], axis=0, keepdims=True)
+            small[b, tap_count + row : tap_count + row + 1, :] = jnp.sum(sums[row, b], axis=0, keepdims=True)
         if b % 2:
             advance()
     flows.insert(0, combine())
@@ -347,16 +375,18 @@
     vmem = pltpu.VMEM
     peers = max(n_dp - 1, 1)
     spec = pl.BlockSpec(memory_space=pltpu.VMEM)
-    grad_value, grad_gate, grad_weight, small = pl.pallas_call(
-        functools.partial(kernel, n_sp, n_dp, plan),
+    grad_value, grad_gate, grad_weight, grad_conv, grad_gain, grad_shift = pl.pallas_call(
+        functools.partial(kernel, n_sp, n_dp, plan, scale),
         out_shape=[
             jax.ShapeDtypeStruct((length, channels), bf16),
             jax.ShapeDtypeStruct((length, channels), bf16),
             jax.ShapeDtypeStruct((local_rows, channels), bf16),
-            jax.ShapeDtypeStruct((small_rows, channels), f32),
+            jax.ShapeDtypeStruct((tap_count, channels), f32),
+            jax.ShapeDtypeStruct((1, channels), f32),
+            jax.ShapeDtypeStruct((1, channels), f32),
         ],
         in_specs=[spec] * 7,
-        out_specs=[spec] * 4,
+        out_specs=[spec] * 6,
         scratch_shapes=[
             vmem((blocks, ext + length, LANES), f32),
             vmem((blocks, length + ext, LANES), f32),
@@ -370,8 +400,9 @@
             vmem((blocks, ext, LANES), f32),
             vmem((blocks, ext, LANES), f32),
             vmem((2, blocks, 8, LANES), f32),
-            vmem((small_rows, channels), f32),
-            vmem((steps, small_rows, channels), f32),
+            vmem((blocks, small_rows, LANES), f32),
+            vmem((steps, blocks, small_rows, LANES), f32),
+            vmem((blocks, small_rows, LANES), f32),
             vmem((peers, streams, stream_rows, channels), f32),
             vmem((peers, streams, stream_rows, channels), f32),
             vmem((streams, stream_rows, channels), f32),
@@ -385,20 +416,19 @@
             dma((3,)), dma((3,)),
             dma((streams, peers)), dma((streams, peers)),
             dma((streams, 2 * len(plan))), dma((streams, 2 * len(plan))),
-            dma((steps,)), dma((steps,)),
+            dma((2 * steps,)), dma((2 * steps,)),
         ],
         compiler_params=pltpu.CompilerParams(
             collective_id=0, has_side_effects=True, vmem_limit_bytes=60 * 1024 * 1024
         ),
     )(glu_value[0], glu_gate[0], cotangent[0], conv_weight, norm_gain[None], norm_shift[None], out_weight)
-    small = small * scale
     return (
         grad_value[None],
         grad_gate[None],
         grad_weight.astype(f32) * scale,
-        small[:tap_count],
-        small[tap_count],
-        small[tap_count + 1],
+        grad_conv,
+        grad_gain[0],
+        grad_shift[0],
     )
 
 

time: 72.8 us -> 68.6 us (0.942)
  Pallas kernels: 65.3 us -> 61.4 us
  other arithmetic: 3.85 us -> 2.92 us
    pallas_call x1, Pallas kernels: 65.3 us -> 61.4 us  [per_device(): pl.pallas_call(functools.partial(kernel, n_sp, n_dp, plan, scale), out_sh...]
    unnamed x6 -> x15, local copies, waits for them, and re-layouts: 1.59 us -> 3.39 us
    slice x2 -> x0, local copies, waits for them, and re-layouts: 1.22 us -> none  [the longest x1 0.63 us: per_device(): small[:tap_count]]
    mul x1 -> x0, other arithmetic: 0.95 us -> none  [per_device(): small = small * scale]
where the time goes in v2:
time: 68.6 us; the launch traced here: 68.4 us
  Pallas kernels  61.4 us (90%)
  local copies, waits for them, and re-layouts  3.39 us (5%)
  other arithmetic  2.92 us (4%)
  between operations  0.69 us (1%)
    pallas_call x1, Pallas kernels, per_device(): pl.pallas_call(functools.partial(kernel, n_sp, n_dp, plan, scale), out_sh...  61.4 us
    unnamed x15, local copies, waits for them, and re-layouts  3.39 us
    mul x1, other arithmetic, per_device(): grad_weight.astype(f32) * scale  2.92 us

profile of v2, /device:TPU:0, one launch (start us, length us, event | category | flops | bytes accessed | tf_op | source)
XLA Modules:
  0.0 68.4 jit_solution(1239853340942421708)
XLA Ops:
  0.6 61.4 %shard_map.118 = (bf16[512,512]{1,0:T(8,128)(2,1)}, bf16[512,512]{1,0:T(8,128)(2,1)}, bf16[1024,512]{1,0:T(8,128)(2,1)}, f32[31,512]{1,0:T(8,128)}, f32[1,512]{1,0:T(1,128)}, /*index=5*/f32[1,512]{1,0:T(1,128)}) custom-call(bf16[512,512]{1,0:T(8,128)(2,1)} %bitcast.10, bf16[512,512]{1,0:T(8,128)(2,1)} %bitcast.11, bf16[512,2048]{1,0:T(8,128)(2,1)} %bitcast.9, ...), custom_call_target="tpu_custom_call" | custom-call | tf_op jit(solution)/shard_map/pallas_call | solution.py:378
  62.1 0.0 copy-start.1
  62.1 0.0 copy-start
  62.1 0.0 copy-start.2
  62.1 0.0 copy-start.4
  62.1 0.0 copy-start.3
  62.1 2.9 %convert_multiply_fusion = f32[1024,512]{1,0:T(8,128)} fusion(bf16[1024,512]{1,0:T(8,128)(2,1)} %get-tuple-element.14), kind=kLoop, calls=%fused_computation | loop fusion | flops 1048576 | bytes 3145728 | tf_op jit(solution)/shard_map/mul | solution.py:428
  65.0 0.0 copy-done.1
  65.0 0.8 %copy.18 = bf16[1,512,512]{2,1,0:T(8,128)(2,1)} copy(bf16[1,512,512]{2,1,0:T(8,128)(2,1)S(1)} %bitcast.13) | data formatting | bytes 1048576
  65.8 0.0 copy-done
  65.8 0.8 %copy.19 = bf16[1,512,512]{2,1,0:T(8,128)(2,1)} copy(bf16[1,512,512]{2,1,0:T(8,128)(2,1)S(1)} %bitcast.12) | data formatting | bytes 1048576
  66.6 0.0 copy-done.2
  66.6 0.6 copy.20
  67.2 0.0 copy-done.4
  67.3 0.6 copy.21
  67.8 0.0 copy-done.3
  67.8 0.6 copy.22
Async XLA Ops:
  62.1 3.0 %copy-start.1 = (bf16[512,512]{1,0:T(8,128)(2,1)S(1)}, bf16[512,512]{1,0:T(8,128)(2,1)}, u32[]{:S(2)}) copy-start(bf16[512,512]{1,0:T(8,128)(2,1)} %get-tuple-element.12) | copy-start | bytes 1572868
  62.1 3.8 %copy-start = (bf16[512,512]{1,0:T(8,128)(2,1)S(1)}, bf16[512,512]{1,0:T(8,128)(2,1)}, u32[]{:S(2)}) copy-start(bf16[512,512]{1,0:T(8,128)(2,1)} %get-tuple-element.13) | copy-start | bytes 1572868
  62.1 4.5 %copy-start.2 = (f32[31,512]{1,0:T(8,128)S(1)}, f32[31,512]{1,0:T(8,128)}, u32[]{:S(2)}) copy-start(f32[31,512]{1,0:T(8,128)} %get-tuple-element.27) | copy-start | bytes 190468
  62.1 5.2 %copy-start.4 = (f32[1,512]{1,0:T(1,128)S(1)}, f32[1,512]{1,0:T(1,128)}, u32[]{:S(2)}) copy-start(f32[1,512]{1,0:T(1,128)} %get-tuple-element.16) | copy-start | bytes 6148
  62.1 5.7 %copy-start.3 = (f32[1,512]{1,0:T(1,128)S(1)}, f32[1,512]{1,0:T(1,128)}, u32[]{:S(2)}) copy-start(f32[1,512]{1,0:T(1,128)} %get-tuple-element.17) | copy-start | bytes 6148

commit v3 on v2

--- a/solution.py
+++ b/solution.py
@@ -13,7 +13,7 @@
 STREAMS = 4
 NARROW_STAGES = 3
 MAX_HALVINGS = 4
-SMALL_HALVINGS = 2
+SMALL_HALVINGS = 1
 f32 = jnp.float32
 bf16 = jnp.bfloat16
 
@@ -264,9 +264,6 @@
             copy.start()
             dp_copies[k][o - 1] = copy
         acc[k] = product(dp, k)
-        if k:
-            next(flows[k - 1])
-    next(flows[streams - 1])
 
     for copy in w_copies:
         copy.wait()
@@ -308,7 +305,6 @@
         return 0
 
     lax.fori_loop(1, row_blocks, backward_loop, 0)
-    advance()
 
     small[...] = jnp.zeros_like(small)
     for b in range(blocks):
@@ -325,8 +321,6 @@
             small[b, j : j + 1, :] = jnp.sum(found[j], axis=0, keepdims=True)
         for row in range(2):
             small[b, tap_count + row : tap_count + row + 1, :] = jnp.sum(sums[row, b], axis=0, keepdims=True)
-        if b % 2:
-            advance()
     flows.insert(0, combine())
     edge.wait()
     for b in range(blocks):

time: 68.6 us -> 63.7 us (0.929)
  Pallas kernels: 61.4 us -> 56.5 us
    pallas_call x1, Pallas kernels: 61.4 us -> 56.5 us  [per_device(): pl.pallas_call(functools.partial(kernel, n_sp, n_dp, plan, scale), out_sh...]
where the time goes in v3:
time: 63.7 us; the launch traced here: 63.5 us
  Pallas kernels  56.5 us (89%)
  local copies, waits for them, and re-layouts  3.39 us (5%)
  other arithmetic  2.92 us (5%)
  between operations  0.69 us (1%)
    pallas_call x1, Pallas kernels, per_device(): pl.pallas_call(functools.partial(kernel, n_sp, n_dp, plan, scale), out_sh...  56.5 us
    unnamed x15, local copies, waits for them, and re-layouts  3.39 us
    mul x1, other arithmetic, per_device(): grad_weight.astype(f32) * scale  2.92 us

profile of v3, /device:TPU:0, one launch (start us, length us, event | category | flops | bytes accessed | tf_op | source)
XLA Modules:
  0.0 63.5 jit_solution(12270914583192536761)
XLA Ops:
  0.6 56.5 %shard_map.118 = (bf16[512,512]{1,0:T(8,128)(2,1)}, bf16[512,512]{1,0:T(8,128)(2,1)}, bf16[1024,512]{1,0:T(8,128)(2,1)}, f32[31,512]{1,0:T(8,128)}, f32[1,512]{1,0:T(1,128)}, /*index=5*/f32[1,512]{1,0:T(1,128)}) custom-call(bf16[512,512]{1,0:T(8,128)(2,1)} %bitcast.10, bf16[512,512]{1,0:T(8,128)(2,1)} %bitcast.11, bf16[512,2048]{1,0:T(8,128)(2,1)} %bitcast.9, ...), custom_call_target="tpu_custom_call" | custom-call | tf_op jit(solution)/shard_map/pallas_call | solution.py:372
  57.2 0.0 copy-start.1
  57.2 0.0 copy-start
  57.2 0.0 copy-start.2
  57.2 0.0 copy-start.4
  57.2 0.0 copy-start.3
  57.2 2.9 %convert_multiply_fusion = f32[1024,512]{1,0:T(8,128)} fusion(bf16[1024,512]{1,0:T(8,128)(2,1)} %get-tuple-element.14), kind=kLoop, calls=%fused_computation | loop fusion | flops 1048576 | bytes 3145728 | tf_op jit(solution)/shard_map/mul | solution.py:422
  60.2 0.0 copy-done.1
  60.2 0.8 %copy.18 = bf16[1,512,512]{2,1,0:T(8,128)(2,1)} copy(bf16[1,512,512]{2,1,0:T(8,128)(2,1)S(1)} %bitcast.13) | data formatting | bytes 1048576
  61.0 0.0 copy-done
  61.0 0.8 %copy.19 = bf16[1,512,512]{2,1,0:T(8,128)(2,1)} copy(bf16[1,512,512]{2,1,0:T(8,128)(2,1)S(1)} %bitcast.12) | data formatting | bytes 1048576
  61.7 0.0 copy-done.2
  61.8 0.6 copy.20
  62.4 0.0 copy-done.4
  62.4 0.6 copy.21
  63.0 0.0 copy-done.3
  63.0 0.6 copy.22
Async XLA Ops:
  57.2 3.0 %copy-start.1 = (bf16[512,512]{1,0:T(8,128)(2,1)S(1)}, bf16[512,512]{1,0:T(8,128)(2,1)}, u32[]{:S(2)}) copy-start(bf16[512,512]{1,0:T(8,128)(2,1)} %get-tuple-element.12) | copy-start | bytes 1572868
  57.2 3.8 %copy-start = (bf16[512,512]{1,0:T(8,128)(2,1)S(1)}, bf16[512,512]{1,0:T(8,128)(2,1)}, u32[]{:S(2)}) copy-start(bf16[512,512]{1,0:T(8,128)(2,1)} %get-tuple-element.13) | copy-start | bytes 1572868
  57.2 4.5 %copy-start.2 = (f32[31,512]{1,0:T(8,128)S(1)}, f32[31,512]{1,0:T(8,128)}, u32[]{:S(2)}) copy-start(f32[31,512]{1,0:T(8,128)} %get-tuple-element.27) | copy-start | bytes 190468
  57.2 5.2 %copy-start.4 = (f32[1,512]{1,0:T(1,128)S(1)}, f32[1,512]{1,0:T(1,128)}, u32[]{:S(2)}) copy-start(f32[1,512]{1,0:T(1,128)} %get-tuple-element.16) | copy-start | bytes 6148
  57.2 5.7 %copy-start.3 = (f32[1,512]{1,0:T(1,128)S(1)}, f32[1,512]{1,0:T(1,128)}, u32[]{:S(2)}) copy-start(f32[1,512]{1,0:T(1,128)} %get-tuple-element.17) | copy-start | bytes 6148

commit v4 on v3

--- a/solution.py
+++ b/solution.py
@@ -273,7 +273,6 @@
         part = jnp.dot(cotan[:, d * local_rows : (d + 1) * local_rows], weights[d], preferred_element_type=f32)
         total = part if total is None else total + part
     grad_act[...] = total
-    advance()
     sums[...] = jnp.zeros_like(sums)
 
     def backward(i):
@@ -299,6 +298,7 @@
     edge_out[...] = grads[:, 0:ext, :]
     edge = remote(edge_out, edge_in, h_send.at[2], h_recv.at[2], {"sp": prior})
     edge.start()
+    advance()
 
     def backward_loop(i, _):
         backward(i)

time: 63.7 us -> 63 us (0.989)
  Pallas kernels: 56.5 us -> 55.8 us
    pallas_call x1, Pallas kernels: 56.5 us -> 55.8 us  [per_device(): pl.pallas_call(functools.partial(kernel, n_sp, n_dp, plan, scale), out_sh...]
where the time goes in v4:
time: 63 us; the launch traced here: 62.8 us
  Pallas kernels  55.8 us (89%)
  local copies, waits for them, and re-layouts  3.39 us (5%)
  other arithmetic  2.92 us (5%)
  between operations  0.69 us (1%)
    pallas_call x1, Pallas kernels, per_device(): pl.pallas_call(functools.partial(kernel, n_sp, n_dp, plan, scale), out_sh...  55.8 us
    unnamed x15, local copies, waits for them, and re-layouts  3.39 us
    mul x1, other arithmetic, per_device(): grad_weight.astype(f32) * scale  2.92 us

profile of v4, /device:TPU:0, one launch (start us, length us, event | category | flops | bytes accessed | tf_op | source)
XLA Modules:
  0.0 62.8 jit_solution(18077768517405930215)
XLA Ops:
  0.6 55.8 %shard_map.118 = (bf16[512,512]{1,0:T(8,128)(2,1)}, bf16[512,512]{1,0:T(8,128)(2,1)}, bf16[1024,512]{1,0:T(8,128)(2,1)}, f32[31,512]{1,0:T(8,128)}, f32[1,512]{1,0:T(1,128)}, /*index=5*/f32[1,512]{1,0:T(1,128)}) custom-call(bf16[512,512]{1,0:T(8,128)(2,1)} %bitcast.10, bf16[512,512]{1,0:T(8,128)(2,1)} %bitcast.11, bf16[512,2048]{1,0:T(8,128)(2,1)} %bitcast.9, ...), custom_call_target="tpu_custom_call" | custom-call | tf_op jit(solution)/shard_map/pallas_call | solution.py:372
  56.5 0.0 copy-start.1
  56.5 0.0 copy-start
  56.5 0.0 copy-start.2
  56.5 0.0 copy-start.4
  56.5 0.0 copy-start.3
  56.5 2.9 %convert_multiply_fusion = f32[1024,512]{1,0:T(8,128)} fusion(bf16[1024,512]{1,0:T(8,128)(2,1)} %get-tuple-element.14), kind=kLoop, calls=%fused_computation | loop fusion | flops 1048576 | bytes 3145728 | tf_op jit(solution)/shard_map/mul | solution.py:422
  59.4 0.0 copy-done.1
  59.4 0.8 %copy.18 = bf16[1,512,512]{2,1,0:T(8,128)(2,1)} copy(bf16[1,512,512]{2,1,0:T(8,128)(2,1)S(1)} %bitcast.13) | data formatting | bytes 1048576
  60.2 0.0 copy-done
  60.2 0.8 %copy.19 = bf16[1,512,512]{2,1,0:T(8,128)(2,1)} copy(bf16[1,512,512]{2,1,0:T(8,128)(2,1)S(1)} %bitcast.12) | data formatting | bytes 1048576
  61.0 0.0 copy-done.2
  61.0 0.6 %copy.20 = f32[31,512]{1,0:T(8,128)} copy(f32[31,512]{1,0:T(8,128)S(1)} %copy-done.2) | data formatting | bytes 126976
  61.6 0.0 copy-done.4
  61.7 0.6 copy.21
  62.2 0.0 copy-done.3
  62.2 0.6 copy.22
Async XLA Ops:
  56.5 3.0 %copy-start.1 = (bf16[512,512]{1,0:T(8,128)(2,1)S(1)}, bf16[512,512]{1,0:T(8,128)(2,1)}, u32[]{:S(2)}) copy-start(bf16[512,512]{1,0:T(8,128)(2,1)} %get-tuple-element.12) | copy-start | bytes 1572868
  56.5 3.8 %copy-start = (bf16[512,512]{1,0:T(8,128)(2,1)S(1)}, bf16[512,512]{1,0:T(8,128)(2,1)}, u32[]{:S(2)}) copy-start(bf16[512,512]{1,0:T(8,128)(2,1)} %get-tuple-element.13) | copy-start | bytes 1572868
  56.5 4.5 %copy-start.2 = (f32[31,512]{1,0:T(8,128)S(1)}, f32[31,512]{1,0:T(8,128)}, u32[]{:S(2)}) copy-start(f32[31,512]{1,0:T(8,128)} %get-tuple-element.27) | copy-start | bytes 190468
  56.5 5.2 %copy-start.4 = (f32[1,512]{1,0:T(1,128)S(1)}, f32[1,512]{1,0:T(1,128)}, u32[]{:S(2)}) copy-start(f32[1,512]{1,0:T(1,128)} %get-tuple-element.16) | copy-start | bytes 6148
  56.5 5.7 %copy-start.3 = (f32[1,512]{1,0:T(1,128)S(1)}, f32[1,512]{1,0:T(1,128)}, u32[]{:S(2)}) copy-start(f32[1,512]{1,0:T(1,128)} %get-tuple-element.17) | copy-start | bytes 6148
